TPU v7x, 128 devices: a whole 4x4x4 slice. The times are simulated.
128 devices in a mesh: ep: 128 (over z, y, x, core).
Axes of the slice: x: 4, y: 4, z: 4, core: 2. Of those that a mesh axis runs over, the one named last changes fastest.
Arguments:
- tokens: bfloat16 [2304, 2048], P('ep'), may hold values from -6 to 6
- attn_norm_gain: float32 [2048], replicated, may hold values from 0.1 to 1.9
- w_query: bfloat16 [2048, 512], replicated, may hold values from -0.125 to 0.125
- w_key: bfloat16 [2048, 128], replicated, may hold values from -0.125 to 0.125
- w_value: bfloat16 [2048, 128], replicated, may hold values from -0.125 to 0.125
- w_forget: bfloat16 [2048, 8], replicated, may hold values from -0.125 to 0.125
- forget_bias: float32 [8], replicated, may hold values from 0.5 to 4
- w_attn_out: bfloat16 [512, 2048], replicated, may hold values from -0.25 to 0.25
- cache_keys: bfloat16 [2304, 1024, 128], P('ep'), may hold values from -72 to 72
- cache_values: bfloat16 [2304, 1024, 128], P('ep'), may hold values from -6 to 6
- cache_logcum: float32 [2304, 8, 1024], P('ep'), as said below
- cache_lengths: int32 [2304], P('ep'), may hold values from 128 to 1024
- expert_norm_gain: float32 [2048], replicated, may hold values from 0.4 to 40
- expert_ids: int32 [2304, 6], P('ep'), may hold values from 0 to 127, all different within a row; in each aligned block of 18 rows (0 to 17, 18 to 35, ...) at most 2 rows name the same one
- expert_weights: float32 [2304, 6], P('ep'), may hold values from 0.1 to 1
- w_expert_gate: bfloat16 [128, 2048, 512], P('ep'), may hold values from -0.125 to 0.125
- w_expert_up: bfloat16 [128, 2048, 512], P('ep'), may hold values from -0.125 to 0.125
- w_expert_down: bfloat16 [128, 512, 2048], P('ep'), may hold values from -0.25 to 0.25
- w_dense_gate: bfloat16 [2048, 4096], P(None, 'ep'), may hold values from -0.125 to 0.125
- w_dense_up: bfloat16 [2048, 4096], P(None, 'ep'), may hold values from -2 to 2
- w_dense_down: bfloat16 [4096, 2048], P('ep'), may hold values from -0.09375 to 0.09375
- dense_norm_gain: float32 [4096], replicated, may hold values from 0.1 to 1.9
- branch_gate: float32 [2048], replicated, may hold values from -0.125 to 0.125
Outputs:
- result: bfloat16 [2304, 2048], P('ep')
Inputs may be any that keep to these rules, and one draw needn't show every extreme that they name: `cache_logcum`: along the positions of each sequence and head the values never rise. `expert_ids`: each row names 6 different experts; among the rows of one device no expert is named by more than 2 rows, and in every draw some device names some expert exactly 2 times.
All inputs are finite; a program needn't handle non-finite values.
Results may differ from a plain program's by a relative error of at most 0.012.
The roundings to bfloat16 on the way count: a program that leaves them out, or rounds other values in their place, can miss the bound.
Values may be sent and summed in bfloat16 or wider, within the bound.
A program may use at most 128 MiB of HBM per device.

v0:
```python
import jax
import jax.numpy as jnp
from jax import lax
from jax.sharding import PartitionSpec as P

HEADS = 8
KV_HEADS = 2
HEAD_DIM = 64
TOPK = 6
EPS = 1e-06
LIMIT = 7.0
ALPHA = 1.702


def normalize(values, gain):
    return values * lax.rsqrt(jnp.mean(values * values, axis=-1, keepdims=True) + EPS) * gain


def stored(values):
    return lax.optimization_barrier(values.astype(jnp.bfloat16))


def attend(
    query, key_new, value_new, log_forget, cache_keys, cache_values, cache_logcum, cache_lengths
):
    seqs, length = (cache_keys.shape[0], cache_keys.shape[1])
    group = HEADS // KV_HEADS
    scale = HEAD_DIM ** (-0.5)
    heads_q = query.reshape(seqs, KV_HEADS, group, HEAD_DIM)
    keys = cache_keys.reshape(seqs, length, KV_HEADS, HEAD_DIM)
    values = cache_values.reshape(seqs, length, KV_HEADS, HEAD_DIM)
    own_key = key_new.reshape(seqs, KV_HEADS, HEAD_DIM)
    own_value = value_new.astype(jnp.float32).reshape(seqs, KV_HEADS, 1, HEAD_DIM)
    last_index = jnp.broadcast_to((cache_lengths - 1)[:, None, None], (seqs, HEADS, 1))
    carried = jnp.take_along_axis(cache_logcum, last_index, axis=2)[:, :, 0] + log_forget
    offset = (carried[:, :, None] - cache_logcum).reshape(seqs, KV_HEADS, group, length)
    scores = (
        jnp.einsum("skgd,slkd->skgl", heads_q, keys, preferred_element_type=jnp.float32) * scale
        + offset
    )
    live = jnp.arange(length, dtype=jnp.int32)[None, :] < cache_lengths[:, None]
    scores = jnp.where(live[:, None, None, :], scores, -jnp.inf)
    own = jnp.einsum("skgd,skd->skg", heads_q, own_key, preferred_element_type=jnp.float32) * scale
    top = jnp.maximum(jnp.max(scores, axis=-1), own)
    expo = jnp.exp(scores - top[..., None])
    own_expo = jnp.exp(own - top)
    total = jnp.sum(expo, axis=-1) + own_expo
    weights = (expo / total[..., None]).astype(jnp.bfloat16)
    own_weight = stored(own_expo / total).astype(jnp.float32)
    out = jnp.einsum("skgl,slkd->skgd", weights, values, preferred_element_type=jnp.float32)
    out = out + own_weight[..., None] * own_value
    return out.reshape(seqs, HEADS * HEAD_DIM).astype(jnp.bfloat16)


def expert_unit(rows, gate_w, up_w, down_w):
    gate = jnp.minimum(jnp.dot(rows, gate_w, preferred_element_type=jnp.float32), LIMIT)
    up = jnp.clip(jnp.dot(rows, up_w, preferred_element_type=jnp.float32), -LIMIT, LIMIT)
    act = ((up + 1.0) * gate * jax.nn.sigmoid(gate * ALPHA)).astype(jnp.bfloat16)
    return jnp.dot(act, down_w, preferred_element_type=jnp.float32).astype(jnp.bfloat16)


def shards(
    tokens,
    attn_norm_gain,
    w_query,
    w_key,
    w_value,
    w_forget,
    forget_bias,
    w_attn_out,
    cache_keys,
    cache_values,
    cache_logcum,
    cache_lengths,
    expert_norm_gain,
    expert_ids,
    expert_weights,
    w_expert_gate,
    w_expert_up,
    w_expert_down,
    w_dense_gate,
    w_dense_up,
    w_dense_down,
    dense_norm_gain,
    branch_gate,
):
    seqs, width = (tokens.shape[0], tokens.shape[1])
    normed = normalize(tokens.astype(jnp.float32), attn_norm_gain).astype(jnp.bfloat16)
    query = jnp.dot(normed, w_query, preferred_element_type=jnp.float32).astype(jnp.bfloat16)
    key_new = jnp.dot(normed, w_key, preferred_element_type=jnp.float32).astype(jnp.bfloat16)
    value_new = jnp.dot(normed, w_value, preferred_element_type=jnp.float32).astype(jnp.bfloat16)
    log_forget = jax.nn.log_sigmoid(
        jnp.dot(normed, w_forget, preferred_element_type=jnp.float32) + forget_bias
    )
    attended = attend(
        query, key_new, value_new, log_forget, cache_keys, cache_values, cache_logcum, cache_lengths
    )
    mixed = stored(
        tokens.astype(jnp.float32)
        + jnp.dot(attended, w_attn_out, preferred_element_type=jnp.float32)
    )
    routed_in = normalize(mixed.astype(jnp.float32), expert_norm_gain).astype(jnp.bfloat16)
    devices = lax.axis_size("ep")
    experts = devices * w_expert_gate.shape[0]
    capacity = max(2, 2 * seqs * TOPK // experts)
    flat_ids = expert_ids.reshape(-1)
    member = (flat_ids[:, None] == jnp.arange(experts, dtype=jnp.int32)[None, :]).astype(jnp.int32)
    slot = jnp.sum(jnp.cumsum(member, axis=0) * member, axis=1) - 1
    target = flat_ids * capacity + slot
    placement = (
        target[:, None] == jnp.arange(experts * capacity, dtype=jnp.int32)[None, :]
    ).astype(jnp.float32)
    per_token = jnp.sum(placement.reshape(seqs, TOPK, experts * capacity), axis=1).astype(
        jnp.bfloat16
    )
    outgoing = jnp.einsum("sc,sd->cd", per_token, routed_in, preferred_element_type=jnp.float32)
    outgoing = outgoing.astype(jnp.bfloat16).reshape(experts, capacity, width)
    arrived = lax.all_to_all(outgoing, "ep", split_axis=0, concat_axis=0, tiled=True)
    count = arrived.shape[1]
    answer = expert_unit(
        arrived.reshape(-1, width), w_expert_gate[0], w_expert_up[0], w_expert_down[0]
    )
    returned = lax.all_to_all(
        answer.reshape(devices, count, width), "ep", split_axis=0, concat_axis=0, tiled=True
    )
    picked = jnp.dot(
        placement.astype(jnp.bfloat16),
        returned.reshape(experts * capacity, width),
        preferred_element_type=jnp.float32,
    )
    routed = jnp.sum(expert_weights[:, :, None] * picked.reshape(seqs, TOPK, width), axis=1)
    piece = lax.all_gather(routed_in, "ep", axis=0, tiled=True)
    gate_dense = jnp.dot(piece, w_dense_gate, preferred_element_type=jnp.float32)
    up_dense = jnp.dot(piece, w_dense_up, preferred_element_type=jnp.float32)
    units = (jax.nn.silu(gate_dense) * up_dense).astype(jnp.bfloat16)
    own_units = lax.all_to_all(units, "ep", split_axis=0, concat_axis=1, tiled=True).astype(
        jnp.float32
    )
    unit_scale = lax.rsqrt(jnp.mean(own_units * own_units, axis=1, keepdims=True) + EPS)
    hidden = (own_units * unit_scale * dense_norm_gain).astype(jnp.bfloat16)
    dense = jnp.dot(
        hidden,
        lax.all_gather(w_dense_down, "ep", axis=0, tiled=True),
        preferred_element_type=jnp.float32,
    )
    branch_scale = jax.nn.sigmoid(
        jnp.sum(routed_in.astype(jnp.float32) * branch_gate, axis=1, keepdims=True)
    )
    return (mixed.astype(jnp.float32) + routed + branch_scale * dense).astype(jnp.bfloat16)


def solution(mesh):
    in_specs = (
        P("ep", None),
        P(),
        P(),
        P(),
        P(),
        P(),
        P(),
        P(),
        P("ep", None, None),
        P("ep", None, None),
        P("ep", None, None),
        P("ep"),
        P(),
        P("ep", None),
        P("ep", None),
        P("ep", None, None),
        P("ep", None, None),
        P("ep", None, None),
        P(None, "ep"),
        P(None, "ep"),
        P("ep", None),
        P(),
        P(),
    )
    out_specs = P("ep", None)
    return jax.shard_map(shards, mesh=mesh, in_specs=in_specs, out_specs=out_specs, check_vma=False)
```

profile of v0, /device:TPU:1, one launch (start us, length us, event | category | flops | bytes accessed | tf_op | source)
XLA Modules:
  0.0 229.7 jit_solution(16532619259781696633)
XLA Ops:
  9.0 5.7 %gather_fusion = f32[144]{0:T(256)S(1)} fusion(f32[18,8,1024]{2,1,0:T(8,128)} %param.33, s32[144]{0:T(256)S(1)} %reshape.290), kind=kCustom, calls=%fused_computation | custom fusion | bytes 2880 | tf_op jit(solution)/shard_map/jit(take_along_axis)/gather | solution.py:35
  17.5 2.0 convolution_convert_fusion.2
  19.7 6.7 %copy.48 = bf16[18,1024,128]{1,2,0:T(8,128)(2,1)} copy(bf16[18,1024,128]{2,1,0:T(8,128)(2,1)} %param.31) | data formatting | bytes 9437184 | tf_op args[8]
  26.9 3.3 %fusion.80 = (f32[18,2,4]{2,1,0:T(2,128)S(1)}, f32[18,2,4,1024]{3,2,1,0:T(4,128)S(1)}) fusion(f32[18,2,4,1024]{3,2,1,0:T(4,128)S(1)} %reshape.279, bf16[18,2,4,64]{3,2,1,0:T(4,128)(2,1)S(1)} %reshape.277, bf16[18,1024,2,64]{1,3,2,0:T(8,128)(2,1)} %bitcast.60, pred[18,1024]{1,0:T(8,128)(4,1)S(1)} %iota_compare_fusion.2), kind=kOutput, calls=%fused_computation.112 | convolution fusion | flops 19464048 | bytes 5935680 | tf_op jit(solution)/shard_map/skgd,slkd->skgl/dot_general | solution.py:38
  31.0 6.6 %copy.52 = bf16[18,1024,128]{1,2,0:T(8,128)(2,1)} copy(bf16[18,1024,128]{2,1,0:T(8,128)(2,1)} %param.32) | data formatting | bytes 9437184 | tf_op args[9]
  37.6 3.7 %fusion.31 = bf16[18,2,4,64]{3,2,1,0:T(4,128)(2,1)S(1)} fusion(bf16[18,1024,2,64]{1,3,2,0:T(8,128)(2,1)} %bitcast.61, f32[18,2,4,1024]{3,2,1,0:T(4,128)S(1)} %get-tuple-element.12, f32[18,2,4]{2,1,0:T(2,128)S(1)} %get-tuple-element.8, f32[18,2,4]{2,1,0:T(2,128)S(1)} %multiply_maximum_fusion, f32[18,2,64]{2,1,0:T(2,128)S(1)} %reshape.286, ...), kind=kOutput, calls=%fused_computation.30 | convolution fusion | flops 19344384 | bytes 5337792 | tf_op jit(solution)/shard_map/skgl,slkd->skgd/dot_general | solution.py:50
  41.5 2.0 fusion.2
  46.6 1.5 reshape.282
  48.2 31.4 %all_to_all.23 = bf16[128,2,2048]{2,1,0:T(2,128)(2,1)S(1)} all-to-all(bf16[128,2,2048]{2,1,0:T(2,128)(2,1)} %reshape.282), channel_id=1, replica_groups=mesh['ep'=128] {'ep'}, dimensions={0} | all-to-all | bytes 2097152 | tf_op jit(solution)/shard_map/all_to_all | solution.py:118
  80.8 3.5 %fusion.16 = f32[256,512]{1,0:T(8,128)} fusion(bf16[256,2048]{1,0:T(8,128)(2,1)} %reshape.283, bf16[1,2048,512]{2,1,0:T(8,128)(2,1)} %param.38), kind=kOutput, calls=%fused_computation.24 | convolution fusion | flops 537001984 | bytes 3670016 | tf_op jit(solution)/shard_map/dot_general | solution.py:56
  84.3 4.1 %convolution_convert_fusion = bf16[256,2048]{1,0:T(8,128)(2,1)} fusion(bf16[1,512,2048]{2,1,0:T(8,128)(2,1)S(1)} %copy-done, f32[256,512]{1,0:T(8,128)} %fusion.16, bf16[256,2048]{1,0:T(8,128)(2,1)S(1)} %copy-done.5, bf16[1,2048,512]{2,1,0:T(8,128)(2,1)} %param.39), kind=kOutput, calls=%fused_computation.3 | convolution fusion | flops 1075445760 | bytes 6815744 | tf_op jit(solution)/shard_map/dot_general | solution.py:59
  88.4 2.6 %reshape.284 = bf16[128,2,2048]{2,1,0:T(2,128)(2,1)} reshape(bf16[256,2048]{1,0:T(8,128)(2,1)} %convolution_convert_fusion) | data formatting | bytes 2097152 | tf_op jit(solution)/shard_map/reshape | solution.py:124
  90.9 4.5 %all-to-all-start.1 = ((bf16[128,2,2048]{2,1,0:T(2,128)(2,1)}), bf16[128,2,2048]{2,1,0:T(2,128)(2,1)S(1)}, u32[]{:S(2)}, u32[]{:S(2)}) async-start(bf16[128,2,2048]{2,1,0:T(2,128)(2,1)} %reshape.284), calls=%async_computation.1 | async-start | bytes 2097152 | tf_op jit(solution)/shard_map/all_to_all | solution.py:123
  95.6 21.0 %all-to-all-done.1 = bf16[128,2,2048]{2,1,0:T(2,128)(2,1)S(1)} async-done(((bf16[128,2,2048]{2,1,0:T(2,128)(2,1)}), bf16[128,2,2048]{2,1,0:T(2,128)(2,1)S(1)}, u32[]{:S(2)}, u32[]{:S(2)}) %all-to-all-start.1) | async-done | bytes 1048608 | tf_op jit(solution)/shard_map/all_to_all | solution.py:123
  117.0 14.3 %all-gather.6.cloned.1.call-done = bf16[128,18,2048]{2,1,0:T(8,128)(2,1)} async-done(((bf16[1,18,2048]{2,1,0:T(8,128)(2,1)}), bf16[128,18,2048]{2,1,0:T(8,128)(2,1)}) %all-gather.6.cloned.1.call-update) | async-done | bytes 9437200 | tf_op jit(solution)/shard_map/all_gather | solution.py:132
  131.3 14.1 %reshape.299 = bf16[2304,2048]{1,0:T(8,128)(2,1)} reshape(bf16[128,18,2048]{2,1,0:T(8,128)(2,1)} %all-gather.6.cloned.1.call-done) | data formatting | bytes 18874368
  145.4 6.8 %fusion.82 = f32[2304,32]{0,1:T(8,128)S(1)} fusion(bf16[2304,2048]{1,0:T(8,128)(2,1)} %reshape.299, bf16[2048,32]{0,1:T(8,128)(2,1)S(1)} %copy-done.8), kind=kOutput, calls=%fused_computation.114 | convolution fusion | flops 301989888 | bytes 9863168 | tf_op jit(solution)/shard_map/dot_general | solution.py:133
  152.2 2.9 %fusion = bf16[2304,32]{0,1:T(8,128)(2,1)S(1)} fusion(bf16[2304,2048]{1,0:T(8,128)(2,1)S(1)} %copy-done.3, bf16[2048,32]{0,1:T(8,128)(2,1)S(1)} %copy-done.9, f32[2304,32]{0,1:T(8,128)S(1)} %fusion.82), kind=kOutput, calls=%fused_computation.2 | convolution fusion | flops 302432256 | bytes 10010624 | tf_op jit(solution)/shard_map/dot_general | solution.py:134
  155.1 2.5 %all_to_all.18 = bf16[128,18,32]{1,0,2:T(8,128)(2,1)S(1)} reshape(bf16[2304,32]{0,1:T(8,128)(2,1)S(1)} %fusion) | data formatting | bytes 294912 | tf_op jit(solution)/shard_map/all_to_all | solution.py:136
  157.7 1.5 copy.56
  160.4 5.8 %all-to-all-start.2 = ((bf16[128,2,288]{2,1,0:T(2,128)(2,1)}), bf16[128,2,288]{2,1,0:T(2,128)(2,1)S(1)}, u32[]{:S(2)}, u32[]{:S(2)}) async-start(bf16[128,2,288]{2,1,0:T(2,128)(2,1)} %reshape.306), calls=%async_computation.2 | async-start | bytes 393216 | tf_op jit(solution)/shard_map/all_to_all | solution.py:136
  166.8 10.8 %all-to-all-done.2 = bf16[128,2,288]{2,1,0:T(2,128)(2,1)S(1)} async-done(((bf16[128,2,288]{2,1,0:T(2,128)(2,1)}), bf16[128,2,288]{2,1,0:T(2,128)(2,1)S(1)}, u32[]{:S(2)}, u32[]{:S(2)}) %all-to-all-start.2) | async-done | bytes 147488 | tf_op jit(solution)/shard_map/all_to_all | solution.py:136
  179.4 34.6 %all-gather.4.cloned.1.call-done = bf16[4096,2048]{1,0:T(8,128)(2,1)} async-done(((bf16[32,2048]{1,0:T(8,128)(2,1)}), bf16[4096,2048]{1,0:T(8,128)(2,1)}) %all-gather.4.cloned.1.call-update) | async-done | bytes 16777232 | tf_op jit(solution)/shard_map/all_gather | solution.py:143
  214.0 8.9 %fusion.3 = bf16[18,2048]{1,0:T(8,128)(2,1)} fusion(bf16[4096,2048]{1,0:T(8,128)(2,1)} %all-gather.4.cloned.1.call-done, f32[18,2048]{1,0:T(8,128)S(1)} %fusion.10, bf16[18,2048]{1,0:T(8,128)(2,1)S(1)} %fusion.2, f32[18,4096]{1,0:T(8,128)S(1)} %reshape.287, f32[4096]{0:T(1024)S(1)} %copy-done.11, f32[18]{0:T(128)S(1)} %add_rsqrt_fusion, ...), kind=kOutput, calls=%fused_computation.10 | convolution fusion | flops 302395392 | bytes 17383568 | tf_op jit(solution)/shard_map/dot_general | solution.py:141
  (94 shorter events, 15.2 us)
Async XLA Ops:
  6.5 77.8 %copy-start = (bf16[1,512,2048]{2,1,0:T(8,128)(2,1)S(1)}, bf16[1,512,2048]{2,1,0:T(8,128)(2,1)}, u32[]{:S(2)}) copy-start(bf16[1,512,2048]{2,1,0:T(8,128)(2,1)} %param.40) | copy-start | bytes 6291460
  6.5 124.8 %all-gather.6.cloned.1.call-start = ((), (), s32[]{:S(2)}) async-start(), calls=%async_computation.4 | async-start | bytes 12681216 | tf_op jit(solution)/shard_map/all_gather | solution.py:132
  9.0 5.9 %copy-start.4 = (bf16[18,2048]{1,0:T(8,128)(2,1)S(1)}, bf16[18,2048]{1,0:T(8,128)(2,1)}, u32[]{:S(2)}) copy-start(bf16[18,2048]{1,0:T(8,128)(2,1)} %param.23) | copy-start | bytes 221188
  9.0 6.0 %copy-start.10 = (f32[2048]{0:T(1024)S(1)}, f32[2048]{0:T(1024)}, u32[]{:S(2)}) copy-start(f32[2048]{0:T(1024)} %param.24) | copy-start | bytes 24580
  9.0 6.0 %copy-start.16 = (bf16[2048,8]{0,1:T(8,128)(2,1)S(1)}, bf16[2048,8]{0,1:T(8,128)(2,1)}, u32[]{:S(2)}) copy-start(bf16[2048,8]{0,1:T(8,128)(2,1)} %param.28) | copy-start | bytes 98308
  9.0 6.0 %copy-start.17 = (f32[8]{0:T(128)S(1)}, f32[8]{0:T(128)}, u32[]{:S(2)}) copy-start(f32[8]{0:T(128)} %param.29) | copy-start | bytes 100
  9.0 6.3 %copy-start.2 = (f32[18,8,1024]{2,1,0:T(8,128)S(1)}, f32[18,8,1024]{2,1,0:T(8,128)}, u32[]{:S(2)}) copy-start(f32[18,8,1024]{2,1,0:T(8,128)} %param.33) | copy-start | bytes 1769476
  19.7 6.7 %copy-start.6 = (bf16[2048,128]{1,0:T(8,128)(2,1)S(1)}, bf16[2048,128]{1,0:T(8,128)(2,1)}, u32[]{:S(2)}) copy-start(bf16[2048,128]{1,0:T(8,128)(2,1)} %param.26) | copy-start | bytes 1572868
  26.9 3.7 %copy-start.7 = (bf16[2048,128]{1,0:T(8,128)(2,1)S(1)}, bf16[2048,128]{1,0:T(8,128)(2,1)}, u32[]{:S(2)}) copy-start(bf16[2048,128]{1,0:T(8,128)(2,1)} %param.27) | copy-start | bytes 1572868
  41.3 2.3 copy-start.12
  41.3 2.3 copy-start.13
  41.3 3.9 %copy-start.14 = (s32[18,6]{0,1:T(8,128)S(1)}, s32[18,6]{0,1:T(8,128)}, u32[]{:S(2)}) copy-start(s32[18,6]{0,1:T(8,128)} %param.36) | copy-start | bytes 1300
  44.5 169.5 %all-gather.4.cloned.1.call-start = ((), (), s32[]{:S(2)}) async-start(), calls=%async_computation.3 | async-start | bytes 16908288 | tf_op jit(solution)/shard_map/all_gather | solution.py:143
  80.8 3.5 %copy-start.5 = (bf16[256,2048]{1,0:T(8,128)(2,1)S(1)}, bf16[256,2048]{1,0:T(8,128)(2,1)}, u32[]{:S(2)}) copy-start(bf16[256,2048]{1,0:T(8,128)(2,1)} %reshape.283) | copy-start | bytes 3145732
  88.4 7.1 %copy-start.15 = (f32[18,6]{0,1:T(8,128)S(1)}, f32[18,6]{0,1:T(8,128)}, u32[]{:S(2)}) copy-start(f32[18,6]{0,1:T(8,128)} %param.37) | copy-start | bytes 1300
  90.9 25.6 %all-to-all-start.1 = ((bf16[128,2,2048]{2,1,0:T(2,128)(2,1)}), bf16[128,2,2048]{2,1,0:T(2,128)(2,1)S(1)}, u32[]{:S(2)}, u32[]{:S(2)}) async-start(bf16[128,2,2048]{2,1,0:T(2,128)(2,1)} %reshape.284), calls=%async_computation.1 | async-start | bytes 2097152 | tf_op jit(solution)/shard_map/all_to_all | solution.py:123
  117.0 28.4 %copy-start.8 = (bf16[2048,32]{0,1:T(8,128)(2,1)S(1)}, bf16[2048,32]{0,1:T(8,128)(2,1)}, u32[]{:S(2)}) copy-start(bf16[2048,32]{0,1:T(8,128)(2,1)} %param.41) | copy-start | bytes 393220
  145.4 6.8 %copy-start.3 = (bf16[2304,2048]{1,0:T(8,128)(2,1)S(1)}, bf16[2304,2048]{1,0:T(8,128)(2,1)}, u32[]{:S(2)}) copy-start(bf16[2304,2048]{1,0:T(8,128)(2,1)} %reshape.299) | copy-start | bytes 28311556
  145.4 6.8 %copy-start.9 = (bf16[2048,32]{0,1:T(8,128)(2,1)S(1)}, bf16[2048,32]{0,1:T(8,128)(2,1)}, u32[]{:S(2)}) copy-start(bf16[2048,32]{0,1:T(8,128)(2,1)} %param.42) | copy-start | bytes 393220
  160.4 17.2 %all-to-all-start.2 = ((bf16[128,2,288]{2,1,0:T(2,128)(2,1)}), bf16[128,2,288]{2,1,0:T(2,128)(2,1)S(1)}, u32[]{:S(2)}, u32[]{:S(2)}) async-start(bf16[128,2,288]{2,1,0:T(2,128)(2,1)} %reshape.306), calls=%async_computation.2 | async-start | bytes 393216 | tf_op jit(solution)/shard_map/all_to_all | solution.py:136
  178.2 35.8 %copy-start.11 = (f32[4096]{0:T(1024)S(1)}, f32[4096]{0:T(1024)}, u32[]{:S(2)}) copy-start(f32[4096]{0:T(1024)} %param.44) | copy-start | bytes 49156
  214.0 8.9 %copy-start.1 = (bf16[1,512,2048]{2,1,0:T(8,128)(2,1)S(1)}, bf16[1,512,2048]{2,1,0:T(8,128)(2,1)}, u32[]{:S(2)}) copy-start(bf16[1,512,2048]{2,1,0:T(8,128)(2,1)} %param.40) | copy-start | bytes 6291460
Sparse Core Ops, SparseCore 0:
  44.6 86.6 all-gather.5
  134.5 79.4 all-gather.3
where the time goes:
time: 231 us; the launch traced here: 230 us
  waiting for transfers between devices  81.3 us (35%)
  local copies, waits for them, and re-layouts  47.9 us (21%)
  matrix products  39.1 us (17%)
  blocking collectives  31.4 us (14%)
  between operations  13.8 us (6%)
  starting transfers between devices  10.4 us (5%)
  other arithmetic  5.76 us (2%)
    all_gather x1, waiting for transfers between devices, shards(): lax.all_gather(w_dense_down, 'ep', axis=0, tiled=True)  34.6 us
    all_to_all x1, blocking collectives, shards(): lax.all_to_all(outgoing, 'ep', split_axis=0, concat_axis=0, tiled=True)  31.4 us
    unnamed x45, local copies, waits for them, and re-layouts  29.5 us
    all_to_all x1, waiting for transfers between devices, shards(): lax.all_to_all(answer.reshape(devices, count, width), 'ep', split_axis=0,...  21 us
    all_gather x1, waiting for transfers between devices, shards(): piece = lax.all_gather(routed_in, 'ep', axis=0, tiled=True)  14.3 us
    all_to_all x1, waiting for transfers between devices, shards(): lax.all_to_all(units, 'ep', split_axis=0, concat_axis=1, tiled=True)  10.8 us
    dot_general x1, matrix products, shards(): jnp.dot(hidden, lax.all_gather(w_dense_down, 'ep', axis=0, tiled=True), p...  8.89 us
    dot_general x1, matrix products, shards(): jnp.dot(piece, w_dense_gate, preferred_element_type=jnp.float32)  6.78 us
  transfers between devices with their start and end apart: 4, of which 4 were waited for; matrix products, arithmetic and copies ran while one was open for 19% of the time, Pallas kernels for 0%

commit v1 on v0

--- a/solution.py
+++ b/solution.py
@@ -10,6 +10,11 @@
 EPS = 1e-06
 LIMIT = 7.0
 ALPHA = 1.702
+
+
+def all_by_exchange(value, mesh_axis, along):
+    repeated = jnp.stack([value] * lax.axis_size(mesh_axis))
+    return jnp.concatenate(lax.all_to_all(repeated, mesh_axis, 0, 0), axis=along)
 
 
 def normalize(values, gain):
@@ -139,9 +144,7 @@
     unit_scale = lax.rsqrt(jnp.mean(own_units * own_units, axis=1, keepdims=True) + EPS)
     hidden = (own_units * unit_scale * dense_norm_gain).astype(jnp.bfloat16)
     dense = jnp.dot(
-        hidden,
-        lax.all_gather(w_dense_down, "ep", axis=0, tiled=True),
-        preferred_element_type=jnp.float32,
+        hidden, all_by_exchange(w_dense_down, "ep", 0), preferred_element_type=jnp.float32
     )
     branch_scale = jax.nn.sigmoid(
         jnp.sum(routed_in.astype(jnp.float32) * branch_gate, axis=1, keepdims=True)

time: 231 us -> 441 us (1.91)
  the two profiles are of different devices: /device:TPU:1 before, /device:TPU:84 now
where the time goes in v1:
time: 441 us; the launch traced here: 440 us
  waiting for transfers between devices  269 us (61%)
  local copies, waits for them, and re-layouts  52.2 us (12%)
  blocking collectives  38.7 us (9%)
  matrix products  38.4 us (9%)
  starting transfers between devices  22 us (5%)
  between operations  13.8 us (3%)
  other arithmetic  5.66 us (1%)
    all_to_all x1, waiting for transfers between devices, all_by_exchange(): lax.all_to_all(repeated, mesh_axis, 0, 0)  237 us
    all_gather x1, waiting for transfers between devices, shards(): piece = lax.all_gather(routed_in, 'ep', axis=0, tiled=True)  31.8 us
    unnamed x47, local copies, waits for them, and re-layouts  28.8 us
    all_to_all x1, blocking collectives, shards(): lax.all_to_all(outgoing, 'ep', split_axis=0, concat_axis=0, tiled=True)  24.6 us
    all_to_all x1, blocking collectives, shards(): lax.all_to_all(units, 'ep', split_axis=0, concat_axis=1, tiled=True)  14.2 us
    all_to_all x1, starting transfers between devices, all_by_exchange(): lax.all_to_all(repeated, mesh_axis, 0, 0)  11.5 us
    all_to_all x1, starting transfers between devices, shards(): lax.all_to_all(answer.reshape(devices, count, width), 'ep', split_axis=0,...  10.4 us
  transfers between devices with their start and end apart: 3, of which 2 were waited for; matrix products, arithmetic and copies ran while one was open for 10% of the time, Pallas kernels for 0%

profile of v1, /device:TPU:84, one launch (start us, length us, event | category | flops | bytes accessed | tf_op | source)
XLA Modules:
  0.0 440.1 jit_solution(17654018630801836910)
XLA Ops:
  9.0 5.4 %gather_fusion = f32[144]{0:T(256)S(1)} fusion(f32[18,8,1024]{2,1,0:T(8,128)} %param.33, s32[144]{0:T(256)S(1)} %reshape.301), kind=kCustom, calls=%fused_computation | custom fusion | bytes 2880 | tf_op jit(solution)/shard_map/jit(take_along_axis)/gather | solution.py:40
  17.3 2.0 convolution_convert_fusion.2
  19.4 6.7 %copy.51 = bf16[18,1024,128]{1,2,0:T(8,128)(2,1)} copy(bf16[18,1024,128]{2,1,0:T(8,128)(2,1)} %param.31) | data formatting | bytes 9437184 | tf_op args[8]
  26.6 3.3 fusion.85
  30.7 6.6 %copy.55 = bf16[18,1024,128]{1,2,0:T(8,128)(2,1)} copy(bf16[18,1024,128]{2,1,0:T(8,128)(2,1)} %param.32) | data formatting | bytes 9437184 | tf_op args[9]
  37.4 3.7 fusion.34
  41.2 2.0 fusion.4
  45.6 1.5 reshape.294
  47.1 24.6 %all_to_all.28 = bf16[128,2,2048]{2,1,0:T(2,128)(2,1)S(1)} all-to-all(bf16[128,2,2048]{2,1,0:T(2,128)(2,1)} %reshape.294), channel_id=1, replica_groups=mesh['ep'=128] {'ep'}, dimensions={0} | all-to-all | bytes 2097152 | tf_op jit(solution)/shard_map/all_to_all | solution.py:123
  73.0 3.5 fusion.19
  76.4 4.1 convolution_convert_fusion
  80.5 2.5 reshape.296
  83.1 10.4 %all-to-all-start.1 = ((bf16[128,2,2048]{2,1,0:T(2,128)(2,1)}), bf16[128,2,2048]{2,1,0:T(2,128)(2,1)S(1)}, u32[]{:S(2)}, u32[]{:S(2)}) async-start(bf16[128,2,2048]{2,1,0:T(2,128)(2,1)} %reshape.296), calls=%async_computation.1 | async-start | bytes 2097152 | tf_op jit(solution)/shard_map/all_to_all | solution.py:128
  93.5 31.8 %all-gather.3.cloned.1.call-done = bf16[128,18,2048]{2,1,0:T(8,128)(2,1)} async-done(((bf16[1,18,2048]{2,1,0:T(8,128)(2,1)}), bf16[128,18,2048]{2,1,0:T(8,128)(2,1)}) %all-gather.3.cloned.1.call-update) | async-done | bytes 9437200 | tf_op jit(solution)/shard_map/all_gather | solution.py:137
  125.4 14.1 %reshape.310 = bf16[2304,2048]{1,0:T(8,128)(2,1)} reshape(bf16[128,18,2048]{2,1,0:T(8,128)(2,1)} %all-gather.3.cloned.1.call-done) | data formatting | bytes 18874368
  139.5 6.7 %fusion.87 = f32[2304,32]{0,1:T(8,128)S(1)} fusion(bf16[2304,2048]{1,0:T(8,128)(2,1)} %reshape.310, bf16[2048,32]{0,1:T(8,128)(2,1)S(1)} %copy-done.8), kind=kOutput, calls=%fused_computation.117 | convolution fusion | flops 301989888 | bytes 9863168 | tf_op jit(solution)/shard_map/dot_general | solution.py:138
  146.2 2.9 fusion
  149.1 2.5 all_to_all.21
  151.6 1.5 copy.59
  153.7 14.2 %all_to_all.29 = bf16[128,2,288]{2,1,0:T(2,128)(2,1)S(1)} all-to-all(bf16[128,2,288]{2,1,0:T(2,128)(2,1)S(1)} %reshape.318), channel_id=1, replica_groups=mesh['ep'=128] {'ep'}, dimensions={0} | all-to-all | bytes 294912 | tf_op jit(solution)/shard_map/all_to_all | solution.py:141
  167.9 6.0 %stack.2 = bf16[128,32,2048]{2,1,0:T(8,128)(2,1)} broadcast(bf16[32,2048]{1,0:T(8,128)(2,1)S(1)} %copy-done.10), dimensions={1,2} | broadcast | bytes 16908288 | tf_op jit(solution)/shard_map/stack | solution.py:16
  173.9 11.5 %all-to-all-start.3 = ((bf16[128,32,2048]{2,1,0:T(8,128)(2,1)}), bf16[128,32,2048]{2,1,0:T(8,128)(2,1)}, u32[]{:S(2)}, u32[]{:S(2)}) async-start(bf16[128,32,2048]{2,1,0:T(8,128)(2,1)} %stack.2), calls=%async_computation.3 | async-start | bytes 33554432 | tf_op jit(solution)/shard_map/all_to_all | solution.py:17
  187.6 237.5 %all-to-all-done.3 = bf16[128,32,2048]{2,1,0:T(8,128)(2,1)} async-done(((bf16[128,32,2048]{2,1,0:T(8,128)(2,1)}), bf16[128,32,2048]{2,1,0:T(8,128)(2,1)}, u32[]{:S(2)}, u32[]{:S(2)}) %all-to-all-start.3) | async-done | bytes 16777248 | tf_op jit(solution)/shard_map/all_to_all | solution.py:17
  425.1 8.2 %fusion.3 = bf16[18,2048]{1,0:T(8,128)(2,1)} fusion(bf16[128,32,2048]{2,1,0:T(8,128)(2,1)} %all-to-all-done.3, bf16[128,18,32]{2,1,0:T(8,128)(2,1)S(1)} %reshape.319, f32[128,32]{1,0:T(8,128)S(1)} %mul.187, f32[18]{0:T(128)S(1)} %add_rsqrt_fusion, f32[18,2048]{1,0:T(8,128)S(1)} %fusion.13, bf16[18,2048]{1,0:T(8,128)(2,1)S(1)} %fusion.4, ...), kind=kOutput, calls=%fused_computation.10 | convolution fusion | flops 302469120 | bytes 17236112 | tf_op jit(solution)/shard_map/dot_general | solution.py:146
  (93 shorter events, 13.0 us)
Async XLA Ops:
  6.5 69.9 %copy-start = (bf16[1,512,2048]{2,1,0:T(8,128)(2,1)S(1)}, bf16[1,512,2048]{2,1,0:T(8,128)(2,1)}, u32[]{:S(2)}) copy-start(bf16[1,512,2048]{2,1,0:T(8,128)(2,1)} %param.40) | copy-start | bytes 6291460
  6.5 118.8 %all-gather.3.cloned.1.call-start = ((), (), s32[]{:S(2)}) async-start(), calls=%async_computation.4 | async-start | bytes 12681216 | tf_op jit(solution)/shard_map/all_gather | solution.py:137
  9.0 5.6 %copy-start.4 = (bf16[18,2048]{1,0:T(8,128)(2,1)S(1)}, bf16[18,2048]{1,0:T(8,128)(2,1)}, u32[]{:S(2)}) copy-start(bf16[18,2048]{1,0:T(8,128)(2,1)} %param.23) | copy-start | bytes 221188
  9.0 5.8 %copy-start.11 = (f32[2048]{0:T(1024)S(1)}, f32[2048]{0:T(1024)}, u32[]{:S(2)}) copy-start(f32[2048]{0:T(1024)} %param.24) | copy-start | bytes 24580
  9.0 5.8 %copy-start.17 = (bf16[2048,8]{0,1:T(8,128)(2,1)S(1)}, bf16[2048,8]{0,1:T(8,128)(2,1)}, u32[]{:S(2)}) copy-start(bf16[2048,8]{0,1:T(8,128)(2,1)} %param.28) | copy-start | bytes 98308
  9.0 5.8 %copy-start.18 = (f32[8]{0:T(128)S(1)}, f32[8]{0:T(128)}, u32[]{:S(2)}) copy-start(f32[8]{0:T(128)} %param.29) | copy-start | bytes 100
  9.0 6.1 %copy-start.2 = (f32[18,8,1024]{2,1,0:T(8,128)S(1)}, f32[18,8,1024]{2,1,0:T(8,128)}, u32[]{:S(2)}) copy-start(f32[18,8,1024]{2,1,0:T(8,128)} %param.33) | copy-start | bytes 1769476
  19.4 6.7 %copy-start.6 = (bf16[2048,128]{1,0:T(8,128)(2,1)S(1)}, bf16[2048,128]{1,0:T(8,128)(2,1)}, u32[]{:S(2)}) copy-start(bf16[2048,128]{1,0:T(8,128)(2,1)} %param.26) | copy-start | bytes 1572868
  26.6 3.7 copy-start.7
  41.1 2.3 copy-start.12
  41.1 2.3 copy-start.14
  41.1 3.2 copy-start.15
  73.0 3.5 copy-start.5
  83.1 70.6 %all-to-all-start.1 = ((bf16[128,2,2048]{2,1,0:T(2,128)(2,1)}), bf16[128,2,2048]{2,1,0:T(2,128)(2,1)S(1)}, u32[]{:S(2)}, u32[]{:S(2)}) async-start(bf16[128,2,2048]{2,1,0:T(2,128)(2,1)} %reshape.296), calls=%async_computation.1 | async-start | bytes 2097152 | tf_op jit(solution)/shard_map/all_to_all | solution.py:128
  93.5 45.9 %copy-start.8 = (bf16[2048,32]{0,1:T(8,128)(2,1)S(1)}, bf16[2048,32]{0,1:T(8,128)(2,1)}, u32[]{:S(2)}) copy-start(bf16[2048,32]{0,1:T(8,128)(2,1)} %param.41) | copy-start | bytes 393220
  139.4 6.7 %copy-start.3 = (bf16[2304,2048]{1,0:T(8,128)(2,1)S(1)}, bf16[2304,2048]{1,0:T(8,128)(2,1)}, u32[]{:S(2)}) copy-start(bf16[2304,2048]{1,0:T(8,128)(2,1)} %reshape.310) | copy-start | bytes 28311556
  139.4 6.8 %copy-start.9 = (bf16[2048,32]{0,1:T(8,128)(2,1)S(1)}, bf16[2048,32]{0,1:T(8,128)(2,1)}, u32[]{:S(2)}) copy-start(bf16[2048,32]{0,1:T(8,128)(2,1)} %param.42) | copy-start | bytes 393220
  149.1 18.8 %copy-start.10 = (bf16[32,2048]{1,0:T(8,128)(2,1)S(1)}, bf16[32,2048]{1,0:T(8,128)(2,1)}, u32[]{:S(2)}) copy-start(bf16[32,2048]{1,0:T(8,128)(2,1)} %param.43) | copy-start | bytes 393220
  173.9 11.5 %copy-start.16 = (f32[18,6]{0,1:T(8,128)S(1)}, f32[18,6]{0,1:T(8,128)}, u32[]{:S(2)}) copy-start(f32[18,6]{0,1:T(8,128)} %param.37) | copy-start | bytes 1300
  173.9 11.6 %copy-start.13 = (f32[4096]{0:T(1024)S(1)}, f32[4096]{0:T(1024)}, u32[]{:S(2)}) copy-start(f32[4096]{0:T(1024)} %param.44) | copy-start | bytes 49156
  173.9 251.2 %all-to-all-start.3 = ((bf16[128,32,2048]{2,1,0:T(8,128)(2,1)}), bf16[128,32,2048]{2,1,0:T(8,128)(2,1)}, u32[]{:S(2)}, u32[]{:S(2)}) async-start(bf16[128,32,2048]{2,1,0:T(8,128)(2,1)} %stack.2), calls=%async_computation.3 | async-start | bytes 33554432 | tf_op jit(solution)/shard_map/all_to_all | solution.py:17
  425.1 8.2 %copy-start.1 = (bf16[1,512,2048]{2,1,0:T(8,128)(2,1)S(1)}, bf16[1,512,2048]{2,1,0:T(8,128)(2,1)}, u32[]{:S(2)}) copy-start(bf16[1,512,2048]{2,1,0:T(8,128)(2,1)} %param.40) | copy-start | bytes 6291460
Sparse Core Ops, SparseCore 0:
  44.4 80.9 all-gather.2
